TPU v7x, 32 devices: a whole 2x2x4 slice. The times are simulated.
32 devices in a mesh: ep: 8 (over z, y), tp: 4 (over x, core).
Axes of the slice: x: 2, y: 2, z: 4, core: 2. Of those that a mesh axis runs over, the one named last changes fastest.
Arguments:
- tokens: bfloat16 [64, 1024], P('ep'), may hold values from -6 to 6
- mix_gain: float32 [1024], replicated, may hold values from 0.1 to 1.9
- w_query: bfloat16 [1024, 512], P(None, 'tp'), may hold values from -0.1875 to 0.1875
- w_key: bfloat16 [1024, 512], P(None, 'tp'), may hold values from -0.1875 to 0.1875
- w_value: bfloat16 [1024, 1024], P(None, 'tp'), may hold values from -0.1875 to 0.1875
- w_ogate: bfloat16 [1024, 1024], P(None, 'tp'), may hold values from -0.1875 to 0.1875
- w_igate: bfloat16 [1024, 4], replicated, may hold values from -0.1875 to 0.1875
- w_fgate: bfloat16 [1024, 4], replicated, may hold values from -0.1875 to 0.1875
- forget_bias: float32 [4], replicated, may hold values from -1 to 3
- head_gain: float32 [1024], P('tp'), may hold values from 0.1 to 1.9
- w_out: bfloat16 [1024, 1024], P('tp'), may hold values from -0.1875 to 0.1875
- memory: float32 [64, 4, 128, 256], P('ep', 'tp'), may hold values from -0.4 to 0.4
- normalizer: float32 [64, 4, 128], P('ep', 'tp'), may hold values from -0.4 to 0.4
- running_max: float32 [64, 4], P('ep', 'tp'), may hold values from -4 to 4
- ffn_gain: float32 [1024], replicated, may hold values from 0.1 to 1.9
- route: int32 [64, 2], replicated, may hold values from 0 to 7, all different within a row; in each aligned block of 64 rows (0 to 63, 64 to 127, ...) at most 32 rows name the same one
- route_weight: float32 [64, 2], replicated, may hold values from 0.05 to 1
- w_gate: bfloat16 [8, 1024, 512], P('ep', None, 'tp'), may hold values from -0.1875 to 0.1875
- w_up: bfloat16 [8, 1024, 512], P('ep', None, 'tp'), may hold values from -0.1875 to 0.1875
- w_down: bfloat16 [8, 512, 1024], P('ep', 'tp'), may hold values from -0.25 to 0.25
Outputs:
- mixed: bfloat16 [64, 1024], P(None, 'ep')
- new_memory: float32 [64, 4, 128, 256], P('ep', 'tp')
- new_normalizer: float32 [64, 4, 128], P('ep', 'tp')
- new_max: float32 [64, 4], P('ep', 'tp')
Inputs may be any that keep to these rules, and one draw needn't show every extreme that they name: `route`: each expert is named by at most 32 routes in all, a bound that some block reaches; the two choices of a token differ.
All inputs are finite; a program needn't handle non-finite values.
Results may differ from a plain program's by a relative error of at most 0.014.
Values may be sent and summed in bfloat16 or wider, within the bound.
No kernel may reach another device: no remote copies, remote signals or barrier semaphores. Data moves between devices by JAX's collectives and lax.ppermute only.
A program may use at most 64 MiB of HBM per device.

v0:
```python
import jax
import jax.numpy as jnp
from jax import lax
from jax.sharding import PartitionSpec as P

EXPERT_CAPACITY = 32
EPS = 1e-06


def round_trip(values):
    rounded = lax.optimization_barrier(values.astype(jnp.bfloat16))
    return rounded.astype(jnp.float32)


def norm_rows(values, gain):
    floats = values.astype(jnp.float32)
    scale = lax.rsqrt(jnp.mean(floats * floats, axis=-1, keepdims=True) + EPS)
    return (floats * scale * gain).astype(jnp.bfloat16)


def slot_targets(route, expert_count, capacity):
    flat = route.reshape(-1)
    onehot = (flat[:, None] == jnp.arange(expert_count, dtype=jnp.int32)[None, :]).astype(jnp.int32)
    before = jnp.cumsum(onehot, axis=0) - onehot
    slot = jnp.sum(before * onehot, axis=1)
    return flat * capacity + slot


def shards(
    tokens,
    mix_gain,
    w_query,
    w_key,
    w_value,
    w_ogate,
    w_igate,
    w_fgate,
    forget_bias,
    head_gain,
    w_out,
    memory,
    normalizer,
    running_max,
    ffn_gain,
    route,
    route_weight,
    w_gate,
    w_up,
    w_down,
):
    width = tokens.shape[1]
    col_count = width // lax.axis_size("ep")
    qk_dim = w_query.shape[1]
    normed = norm_rows(tokens, mix_gain)
    query = round_trip(jnp.dot(normed, w_query, preferred_element_type=jnp.float32))
    scaled_key = round_trip(
        jnp.dot(normed, w_key, preferred_element_type=jnp.float32)
    ) * qk_dim ** (-0.5)
    value = round_trip(jnp.dot(normed, w_value, preferred_element_type=jnp.float32))
    ogate = round_trip(jnp.dot(normed, w_ogate, preferred_element_type=jnp.float32))
    head_pick = (jnp.arange(w_igate.shape[1], dtype=jnp.int32) == lax.axis_index("tp")).astype(
        jnp.float32
    )
    log_in = jnp.sum(
        jnp.dot(normed, w_igate, preferred_element_type=jnp.float32) * head_pick, axis=1
    )
    forget_pre = jnp.sum(
        jnp.dot(normed, w_fgate, preferred_element_type=jnp.float32) * head_pick, axis=1
    )
    log_forget = jax.nn.log_sigmoid(forget_pre + jnp.sum(forget_bias * head_pick))
    old_max = running_max[:, 0]
    new_max = jnp.maximum(log_forget + old_max, log_in)
    keep = jnp.exp(log_forget + old_max - new_max)
    admit = jnp.exp(log_in - new_max)
    state = (
        keep[:, None, None] * memory[:, 0]
        + admit[:, None, None] * scaled_key[:, :, None] * value[:, None, :]
    )
    norm_state = keep[:, None] * normalizer[:, 0] + admit[:, None] * scaled_key
    numer = jnp.einsum("tk,tkv->tv", query, state, precision=lax.Precision.HIGHEST)
    denom = jnp.sum(query * norm_state, axis=1)
    read = numer / jnp.maximum(jnp.abs(denom), jnp.exp(-new_max))[:, None]
    scale = lax.rsqrt(jnp.mean(read * read, axis=-1, keepdims=True) + EPS)
    gated = (jax.nn.sigmoid(ogate) * read * scale * head_gain).astype(jnp.bfloat16)
    local_output = lax.psum(
        jnp.dot(gated, w_out, preferred_element_type=jnp.float32).astype(jnp.bfloat16), "tp"
    ).astype(jnp.float32)
    middle_rows = (tokens.astype(jnp.float32) + local_output).astype(jnp.bfloat16)
    middle = lax.all_to_all(middle_rows, "ep", split_axis=1, concat_axis=0, tiled=True)
    expert_count = w_gate.shape[0] * lax.axis_size("ep")
    topk_count = route.shape[1]
    targets = slot_targets(route, expert_count, EXPERT_CAPACITY)
    buffer = (
        jnp.zeros((expert_count * EXPERT_CAPACITY, col_count), jnp.bfloat16)
        .at[targets]
        .set(jnp.repeat(middle, topk_count, axis=0))
    )
    buffer = buffer.reshape(expert_count, EXPERT_CAPACITY, col_count)
    rows = lax.all_to_all(buffer, "ep", split_axis=0, concat_axis=2, tiled=True)
    rows = norm_rows(rows, ffn_gain)
    gate_v = jnp.einsum("ecd,edf->ecf", rows, w_gate, preferred_element_type=jnp.float32)
    up_v = jnp.einsum("ecd,edf->ecf", rows, w_up, preferred_element_type=jnp.float32)
    activation = (jax.nn.silu(gate_v) * up_v).astype(jnp.bfloat16)
    partial_value = jnp.einsum(
        "ecf,efd->ecd", activation, w_down, preferred_element_type=jnp.float32
    )
    results = lax.psum(partial_value.astype(jnp.bfloat16), "tp")
    returned = lax.all_to_all(results, "ep", split_axis=2, concat_axis=0, tiled=True)
    picked = returned.reshape(expert_count * EXPERT_CAPACITY, col_count)[targets]
    picked = picked.reshape(route.shape[0], topk_count, col_count).astype(jnp.float32)
    weights = route_weight / jnp.sum(route_weight, axis=1, keepdims=True)
    mixed = (middle.astype(jnp.float32) + jnp.sum(picked * weights[:, :, None], axis=1)).astype(
        jnp.bfloat16
    )
    return (mixed, state[:, None], norm_state[:, None], new_max[:, None])


def solution(mesh):
    return jax.shard_map(
        shards,
        mesh=mesh,
        in_specs=(
            P("ep", None),
            P(),
            P(None, "tp"),
            P(None, "tp"),
            P(None, "tp"),
            P(None, "tp"),
            P(),
            P(),
            P(),
            P("tp"),
            P("tp", None),
            P("ep", "tp", None, None),
            P("ep", "tp", None),
            P("ep", "tp"),
            P(),
            P(),
            P(),
            P("ep", None, "tp"),
            P("ep", None, "tp"),
            P("ep", "tp", None),
        ),
        out_specs=(P(None, "ep"), P("ep", "tp", None, None), P("ep", "tp", None), P("ep", "tp")),
        check_vma=False,
    )
```

profile of v0, /device:TPU:0, one launch (start us, length us, event | category | flops | bytes accessed | tf_op | source)
XLA Modules:
  0.0 114.8 jit_solution(4171381798939121330)
XLA Ops:
  7.2 1.4 %fusion.48 = f32[]{:T(128)} fusion(f32[4]{0:T(128)} %param.28, s32[]{:T(128)S(6)} %axis_index.12), kind=kLoop, calls=%fused_computation.81 | loop fusion | flops 11 | bytes 24 | tf_op jit(solution)/shard_map/reduce_sum | solution.py:70
  8.7 0.8 fusion.28
  9.5 0.9 fusion.3
  10.4 0.9 fusion.2
  11.3 1.3 %fusion.46 = (f32[8]{0:T(128)S(1)}, f32[8]{0:T(128)S(1)}) fusion(f32[8]{0:T(128)S(1)} %fusion.3, f32[8,1]{0,1:T(1,128)} %param.33, f32[8]{0:T(128)S(1)} %fusion.2, f32[]{:T(128)} %fusion.48), kind=kLoop, calls=%fused_computation.79 | loop fusion | flops 96 | bytes 164 | tf_op jit(solution)/shard_map/exp | solution.py:73
  12.7 1.3 %exponential_bitcast_fusion = (f32[8]{0:T(128)S(1)}, f32[8,1]{0,1:T(1,128)S(1)}) fusion(f32[8]{0:T(128)S(1)} %fusion.3, f32[8,1]{0,1:T(1,128)} %param.33, f32[8]{0:T(128)S(1)} %fusion.2, f32[]{:T(128)} %fusion.48), kind=kLoop, calls=%fused_computation.104 | loop fusion | flops 96 | bytes 164 | tf_op jit(solution)/shard_map/mul | solution.py:79
  14.1 0.9 convolution_convert_fusion.5
  14.9 1.2 %convolution_convert_fusion.4 = bf16[8,128]{1,0:T(8,128)(2,1)S(1)} fusion(bf16[1024,128]{1,0:T(8,128)(2,1)} %param.23, bf16[8,1024]{1,0:T(8,128)(2,1)S(1)} %copy-done.3, f32[1024]{0:T(1024)} %param.21, f32[8]{0:T(128)S(1)} %add_rsqrt_fusion.2), kind=kOutput, calls=%fused_computation.9 | convolution fusion | flops 2130944 | bytes 284704 | tf_op jit(solution)/shard_map/dot_general | solution.py:57
  16.1 0.9 convolution_convert_fusion.2
  17.0 1.3 %convolution_convert_fusion.3 = bf16[8,256]{1,0:T(8,128)(2,1)S(1)} fusion(bf16[1024,256]{1,0:T(8,128)(2,1)} %param.25, bf16[8,1024]{1,0:T(8,128)(2,1)S(1)} %copy-done.3, f32[1024]{0:T(1024)} %param.21, f32[8]{0:T(128)S(1)} %add_rsqrt_fusion.2), kind=kOutput, calls=%fused_computation.8 | convolution fusion | flops 4229120 | bytes 548896 | tf_op jit(solution)/shard_map/dot_general | solution.py:60
  18.3 0.7 copy-done.10
  19.0 0.8 multiply_reduce_fusion.1
  19.8 0.6 fusion.5
  20.4 0.2 multiply_reduce_fusion
  20.6 0.7 copy-done.13
  21.3 0.2 convolution_convert_fusion.1
  21.5 12.7 %psum.14 = bf16[8,1024]{1,0:T(8,128)(2,1)S(1)} all-reduce(bf16[8,1024]{1,0:T(8,128)(2,1)S(1)} %convolution_convert_fusion.1), channel_id=1, replica_groups=mesh['ep'=8,'tp'=4] {'tp'}, use_global_device_ids=true, to_apply=%region_6.7 | all-reduce | flops 8192 | bytes 32768 | tf_op jit(solution)/shard_map/psum | solution.py:85
  34.2 0.6 fusion.34
  34.8 6.0 %all-to-all-start = ((bf16[8,8,128]{2,0,1:T(8,128)(2,1)}), bf16[8,8,128]{2,0,1:T(8,128)(2,1)S(1)}, u32[]{:S(2)}, u32[]{:S(2)}) async-start(bf16[8,8,128]{2,0,1:T(8,128)(2,1)} %fusion.34), calls=%async_computation | async-start | bytes 32768 | tf_op jit(solution)/shard_map/all_to_all | solution.py:89
  40.8 0.1 copy.48
  40.9 0.1 copy.47
  41.0 0.1 mul.253
  41.2 0.1 eq.27
  41.4 0.2 reduce_window_sum.11
  41.6 0.2 select_reduce_fusion
  41.8 5.6 %all-to-all-done = bf16[8,8,128]{2,0,1:T(8,128)(2,1)S(1)} async-done(((bf16[8,8,128]{2,0,1:T(8,128)(2,1)}), bf16[8,8,128]{2,0,1:T(8,128)(2,1)S(1)}, u32[]{:S(2)}, u32[]{:S(2)}) %all-to-all-start) | async-done | bytes 16416 | tf_op jit(solution)/shard_map/all_to_all | solution.py:89
  47.4 0.9 scatter_custom_fusion
  48.3 9.3 %all_to_all.43 = bf16[8,32,128]{2,1,0:T(8,128)(2,1)S(1)} all-to-all(bf16[8,32,128]{2,1,0:T(8,128)(2,1)S(1)} %bitcast.126), channel_id=1, replica_groups=mesh['ep'=8,'tp'=4] {'ep'}, dimensions={0} | all-to-all | bytes 131072 | tf_op jit(solution)/shard_map/all_to_all | solution.py:99
  57.6 0.1 fusion.16
  57.7 0.6 copy-done.7
  58.4 0.2 fusion.14
  58.6 0.6 copy-done.6
  59.2 0.1 copy-done.5
  59.3 0.9 fusion
  60.3 1.2 %multiply_add_fusion = f32[8,1,128,256]{3,2,1,0:T(8,128)} fusion(f32[8,1,128,256]{3,2,1,0:T(8,128)S(1)} %copy-done.1, f32[8,256]{1,0:T(8,128)S(1)} %convert_element_type.117, f32[8,128]{1,0:T(8,128)S(1)} %get-tuple-element.30, f32[8]{0:T(128)S(1)} %get-tuple-element.24), kind=kLoop, calls=%fused_computation.18 | loop fusion | flops 786432 | bytes 2109472 | tf_op jit(solution)/shard_map/add | solution.py:76
  61.5 27.0 %all-reduce.2.cloned.1.call-done = bf16[1,32,1024]{2,1,0:T(8,128)(2,1)} async-done(((bf16[1,32,1024]{2,1,0:T(8,128)(2,1)}), bf16[1,32,1024]{2,1,0:T(8,128)(2,1)}) %all-reduce.2.cloned.1.call-update) | async-done | bytes 65552 | tf_op jit(solution)/shard_map/psum | solution.py:107
  88.5 1.1 copy.50
  89.6 0.5 broadcast.215
  90.1 2.3 %reduce.3 = bf16[1024,32]{1,0:T(8,128)(2,1)S(1)} reduce(bf16[1024,1,32]{2,1,0:T(2,128)(2,1)S(1)} %bitcast.121, bf16[]{:T(256)} %broadcast.215), dimensions={1}, to_apply=%bitcast.105.reduce_sub_computation | reduce | bytes 131074
  92.4 0.9 reshape.303
  93.3 5.5 %all-to-all-start.2 = ((bf16[8,2,2048]{2,1,0:T(2,128)(2,1)}), bf16[8,2,2048]{2,1,0:T(2,128)(2,1)S(1)}, u32[]{:S(2)}, u32[]{:S(2)}) async-start(bf16[8,2,2048]{2,1,0:T(2,128)(2,1)} %reshape.303), calls=%async_computation.2 | async-start | bytes 131072 | tf_op jit(solution)/shard_map/all_to_all | solution.py:108
  98.8 0.1 copy.53
  99.0 6.8 %all-to-all-done.2 = bf16[8,2,2048]{2,1,0:T(2,128)(2,1)S(1)} async-done(((bf16[8,2,2048]{2,1,0:T(2,128)(2,1)}), bf16[8,2,2048]{2,1,0:T(2,128)(2,1)S(1)}, u32[]{:S(2)}, u32[]{:S(2)}) %all-to-all-start.2) | async-done | bytes 65568 | tf_op jit(solution)/shard_map/all_to_all | solution.py:108
  105.7 0.3 reshape.304
  106.1 0.3 copy.51
  106.4 0.7 gather_fusion
  107.2 0.1 fusion.23
  107.3 0.6 add_convert_fusion
  (45 shorter events, 0.5 us)
Async XLA Ops:
  7.2 13.5 %copy-start = (bf16[256,1024]{1,0:T(8,128)(2,1)S(1)}, bf16[256,1024]{1,0:T(8,128)(2,1)}, u32[]{:S(2)}) copy-start(bf16[256,1024]{1,0:T(8,128)(2,1)} %param.30) | copy-start | bytes 1572868
  7.2 2.3 %copy-start.3 = (bf16[8,1024]{1,0:T(8,128)(2,1)S(1)}, bf16[8,1024]{1,0:T(8,128)(2,1)}, u32[]{:S(2)}) copy-start(bf16[8,1024]{1,0:T(8,128)(2,1)} %param.20) | copy-start | bytes 49156
  7.2 6.8 %copy-start.12 = (bf16[1024,128]{1,0:T(8,128)(2,1)S(1)}, bf16[1024,128]{1,0:T(8,128)(2,1)}, u32[]{:S(2)}) copy-start(bf16[1024,128]{1,0:T(8,128)(2,1)} %param.22) | copy-start | bytes 786436
  7.2 8.9 %copy-start.2 = (bf16[1024,256]{1,0:T(8,128)(2,1)S(1)}, bf16[1024,256]{1,0:T(8,128)(2,1)}, u32[]{:S(2)}) copy-start(bf16[1024,256]{1,0:T(8,128)(2,1)} %param.24) | copy-start | bytes 1572868
  7.2 12.6 %copy-start.1 = (f32[8,1,128,256]{3,2,1,0:T(8,128)S(1)}, f32[8,1,128,256]{3,2,1,0:T(8,128)}, u32[]{:S(2)}) copy-start(f32[8,1,128,256]{3,2,1,0:T(8,128)} %param.31) | copy-start | bytes 3145732
  14.0 5.8 %copy-start.11 = (f32[8,1]{0,1:T(1,128)}, f32[8,1]{0,1:T(1,128)S(1)}, u32[]{:S(2)}) copy-start(f32[8,1]{0,1:T(1,128)S(1)} %get-tuple-element.29) | copy-start | bytes 100
  18.3 0.7 copy-start.10
  20.6 0.7 copy-start.13
  34.8 6.0 %copy-start.8 = (s32[64,2]{0,1:T(2,128)S(1)}, s32[64,2]{0,1:T(2,128)}, u32[]{:S(2)}) copy-start(s32[64,2]{0,1:T(2,128)} %param.35) | copy-start | bytes 1540
  34.8 12.5 %all-to-all-start = ((bf16[8,8,128]{2,0,1:T(8,128)(2,1)}), bf16[8,8,128]{2,0,1:T(8,128)(2,1)S(1)}, u32[]{:S(2)}, u32[]{:S(2)}) async-start(bf16[8,8,128]{2,0,1:T(8,128)(2,1)} %fusion.34), calls=%async_computation | async-start | bytes 32768 | tf_op jit(solution)/shard_map/all_to_all | solution.py:89
  40.8 47.7 %all-reduce.2.cloned.1.call-start = ((), (), s32[]{:S(2)}) async-start(), calls=%async_computation.3 | async-start | bytes 131072 | tf_op jit(solution)/shard_map/psum | solution.py:107
  47.4 11.0 %copy-start.4 = (bf16[1,1024,128]{2,1,0:T(8,128)(2,1)S(1)}, bf16[1,1024,128]{2,1,0:T(8,128)(2,1)}, u32[]{:S(2)}) copy-start(bf16[1,1024,128]{2,1,0:T(8,128)(2,1)} %param.37) | copy-start | bytes 786436
  57.6 0.7 copy-start.7
  58.3 0.9 copy-start.6
  58.4 1.0 copy-start.5
  60.3 1.2 %copy-start.9 = (f32[64,2]{0,1:T(2,128)S(1)}, f32[64,2]{0,1:T(2,128)}, u32[]{:S(2)}) copy-start(f32[64,2]{0,1:T(2,128)} %param.36) | copy-start | bytes 1540
  93.3 12.4 %all-to-all-start.2 = ((bf16[8,2,2048]{2,1,0:T(2,128)(2,1)}), bf16[8,2,2048]{2,1,0:T(2,128)(2,1)S(1)}, u32[]{:S(2)}, u32[]{:S(2)}) async-start(bf16[8,2,2048]{2,1,0:T(2,128)(2,1)} %reshape.303), calls=%async_computation.2 | async-start | bytes 131072 | tf_op jit(solution)/shard_map/all_to_all | solution.py:108
Sparse Core Ops, SparseCore 0:
  60.4 28.0 all-reduce.1
where the time goes:
time: 116 us; the launch traced here: 115 us
  waiting for transfers between devices  39.4 us (34%)
  blocking collectives  22 us (19%)
  between operations  14.3 us (12%)
  starting transfers between devices  11.5 us (10%)
  other arithmetic  11.4 us (10%)
  local copies, waits for them, and re-layouts  8.14 us (7%)
  matrix products  7.98 us (7%)
    psum x1, waiting for transfers between devices, shards(): results = lax.psum(partial_value.astype(jnp.bfloat16), 'tp')  27 us
    psum x1, blocking collectives, shards(): lax.psum(jnp.dot(gated, w_out, preferred_element_type=jnp.float32).astype...  12.7 us
    all_to_all x1, blocking collectives, shards(): rows = lax.all_to_all(buffer, 'ep', split_axis=0, concat_axis=2, tiled=True)  9.29 us
    all_to_all x1, waiting for transfers between devices, shards(): lax.all_to_all(results, 'ep', split_axis=2, concat_axis=0, tiled=True)  6.79 us
    all_to_all x1, starting transfers between devices, shards(): lax.all_to_all(middle_rows, 'ep', split_axis=1, concat_axis=0, tiled=True)  5.97 us
    all_to_all x1, waiting for transfers between devices, shards(): lax.all_to_all(middle_rows, 'ep', split_axis=1, concat_axis=0, tiled=True)  5.58 us
    all_to_all x1, starting transfers between devices, shards(): lax.all_to_all(results, 'ep', split_axis=2, concat_axis=0, tiled=True)  5.52 us
    unnamed x33, local copies, waits for them, and re-layouts  4.59 us
  transfers between devices with their start and end apart: 3, of which 3 were waited for; matrix products, arithmetic and copies ran while one was open for 2% of the time, Pallas kernels for 0%

commit v1 on v0

--- a/solution.py
+++ b/solution.py
@@ -86,7 +86,10 @@
         jnp.dot(gated, w_out, preferred_element_type=jnp.float32).astype(jnp.bfloat16), "tp"
     ).astype(jnp.float32)
     middle_rows = (tokens.astype(jnp.float32) + local_output).astype(jnp.bfloat16)
-    middle = lax.all_to_all(middle_rows, "ep", split_axis=1, concat_axis=0, tiled=True)
+    peers = lax.axis_size("ep")
+    shards_2 = jnp.stack(jnp.split(middle_rows, peers, axis=1), axis=0)
+    shards_2 = lax.all_to_all(shards_2, "ep", split_axis=0, concat_axis=0)
+    middle = jnp.concatenate(shards_2, axis=0)
     expert_count = w_gate.shape[0] * lax.axis_size("ep")
     topk_count = route.shape[1]
     targets = slot_targets(route, expert_count, EXPERT_CAPACITY)

time: 116 us -> 120 us (1.034)
  local copies, waits for them, and re-layouts: 8.14 us -> 12.8 us
    unnamed x33 -> x40, local copies, waits for them, and re-layouts: 4.59 us -> 8.64 us
where the time goes in v1:
time: 120 us; the launch traced here: 119 us
  waiting for transfers between devices  39.4 us (33%)
  blocking collectives  22 us (18%)
  between operations  14.3 us (12%)
  local copies, waits for them, and re-layouts  12.8 us (11%)
  starting transfers between devices  11.5 us (10%)
  other arithmetic  10.8 us (9%)
  matrix products  7.98 us (7%)
    psum x1, waiting for transfers between devices, shards(): results = lax.psum(partial_value.astype(jnp.bfloat16), 'tp')  27 us
    psum x1, blocking collectives, shards(): lax.psum(jnp.dot(gated, w_out, preferred_element_type=jnp.float32).astype...  12.7 us
    all_to_all x1, blocking collectives, shards(): rows = lax.all_to_all(buffer, 'ep', split_axis=0, concat_axis=2, tiled=True)  9.29 us
    unnamed x40, local copies, waits for them, and re-layouts  8.64 us
    all_to_all x1, waiting for transfers between devices, shards(): lax.all_to_all(results, 'ep', split_axis=2, concat_axis=0, tiled=True)  6.79 us
    all_to_all x1, starting transfers between devices, shards(): shards_2 = lax.all_to_all(shards_2, 'ep', split_axis=0, concat_axis=0)  5.97 us
    all_to_all x1, waiting for transfers between devices, shards(): shards_2 = lax.all_to_all(shards_2, 'ep', split_axis=0, concat_axis=0)  5.58 us
    all_to_all x1, starting transfers between devices, shards(): lax.all_to_all(results, 'ep', split_axis=2, concat_axis=0, tiled=True)  5.52 us
  transfers between devices with their start and end apart: 3, of which 3 were waited for; matrix products, arithmetic and copies ran while one was open for 2% of the time, Pallas kernels for 0%

profile of v1, /device:TPU:0, one launch (start us, length us, event | category | flops | bytes accessed | tf_op | source)
XLA Modules:
  0.0 118.8 jit_solution(5787094880206951014)
XLA Ops:
  7.2 1.4 %fusion.47 = f32[]{:T(128)} fusion(f32[4]{0:T(128)} %param.28, s32[]{:T(128)S(6)} %axis_index.12), kind=kLoop, calls=%fused_computation.96 | loop fusion | flops 11 | bytes 24 | tf_op jit(solution)/shard_map/reduce_sum | solution.py:70
  8.7 0.8 fusion.28
  9.5 0.9 fusion.3
  10.4 0.9 fusion.2
  11.3 1.3 %fusion.45 = (f32[8]{0:T(128)S(1)}, f32[8]{0:T(128)S(1)}) fusion(f32[8]{0:T(128)S(1)} %fusion.3, f32[8,1]{0,1:T(1,128)} %param.33, f32[8]{0:T(128)S(1)} %fusion.2, f32[]{:T(128)} %fusion.47), kind=kLoop, calls=%fused_computation.94 | loop fusion | flops 96 | bytes 164 | tf_op jit(solution)/shard_map/exp | solution.py:73
  12.7 1.3 %exponential_bitcast_fusion = (f32[8]{0:T(128)S(1)}, f32[8,1]{0,1:T(1,128)S(1)}) fusion(f32[8]{0:T(128)S(1)} %fusion.3, f32[8,1]{0,1:T(1,128)} %param.33, f32[8]{0:T(128)S(1)} %fusion.2, f32[]{:T(128)} %fusion.47), kind=kLoop, calls=%fused_computation.119 | loop fusion | flops 96 | bytes 164 | tf_op jit(solution)/shard_map/mul | solution.py:79
  14.1 0.9 convolution_convert_fusion.5
  14.9 1.2 convolution_convert_fusion.4
  16.1 0.9 convolution_convert_fusion.2
  17.0 1.3 %convolution_convert_fusion.3 = bf16[8,256]{1,0:T(8,128)(2,1)S(1)} fusion(bf16[1024,256]{1,0:T(8,128)(2,1)} %param.25, bf16[8,1024]{1,0:T(8,128)(2,1)S(1)} %copy-done.3, f32[1024]{0:T(1024)} %param.21, f32[8]{0:T(128)S(1)} %add_rsqrt_fusion.2), kind=kOutput, calls=%fused_computation.8 | convolution fusion | flops 4229120 | bytes 548896 | tf_op jit(solution)/shard_map/dot_general | solution.py:60
  18.3 0.7 copy-done.10
  19.0 0.8 multiply_reduce_fusion.1
  19.8 0.6 fusion.5
  20.4 0.2 multiply_reduce_fusion
  20.6 0.7 copy-done.13
  21.3 0.2 convolution_convert_fusion.1
  21.5 12.7 %psum.14 = bf16[8,1024]{1,0:T(8,128)(2,1)S(1)} all-reduce(bf16[8,1024]{1,0:T(8,128)(2,1)S(1)} %convolution_convert_fusion.1), channel_id=1, replica_groups=mesh['ep'=8,'tp'=4] {'tp'}, use_global_device_ids=true, to_apply=%region_6.7 | all-reduce | flops 8192 | bytes 32768 | tf_op jit(solution)/shard_map/psum | solution.py:85
  34.2 0.6 constant_dynamic-update-slice_fusion.7
  34.8 0.6 constant_dynamic-update-slice_fusion.6
  35.4 0.6 constant_dynamic-update-slice_fusion.5
  35.9 0.6 constant_dynamic-update-slice_fusion.4
  36.5 0.6 constant_dynamic-update-slice_fusion.3
  37.1 0.6 constant_dynamic-update-slice_fusion.2
  37.7 0.6 constant_dynamic-update-slice_fusion.1
  38.3 0.6 constant_dynamic-update-slice_fusion
  38.8 6.0 %all-to-all-start = ((bf16[8,8,128]{2,1,0:T(8,128)(2,1)}), bf16[8,8,128]{2,1,0:T(8,128)(2,1)S(1)}, u32[]{:S(2)}, u32[]{:S(2)}) async-start(bf16[8,8,128]{2,1,0:T(8,128)(2,1)} %constant_dynamic-update-slice_fusion), calls=%async_computation | async-start | bytes 32768 | tf_op jit(solution)/shard_map/all_to_all | solution.py:91
  45.4 0.2 reduce_window_sum.11
  45.6 0.2 select_reduce_fusion
  45.8 5.6 %all-to-all-done = bf16[8,8,128]{2,1,0:T(8,128)(2,1)S(1)} async-done(((bf16[8,8,128]{2,1,0:T(8,128)(2,1)}), bf16[8,8,128]{2,1,0:T(8,128)(2,1)S(1)}, u32[]{:S(2)}, u32[]{:S(2)}) %all-to-all-start) | async-done | bytes 16416 | tf_op jit(solution)/shard_map/all_to_all | solution.py:91
  51.4 0.9 scatter_custom_fusion
  52.3 9.3 %all_to_all.29 = bf16[8,32,128]{2,1,0:T(8,128)(2,1)S(1)} all-to-all(bf16[8,32,128]{2,1,0:T(8,128)(2,1)S(1)} %bitcast.154), channel_id=1, replica_groups=mesh['ep'=8,'tp'=4] {'ep'}, dimensions={0} | all-to-all | bytes 131072 | tf_op jit(solution)/shard_map/all_to_all | solution.py:102
  61.7 0.6 copy-done.7
  62.5 0.2 fusion.14
  62.6 0.6 copy-done.6
  63.4 0.9 fusion
  64.3 1.2 multiply_add_fusion
  65.5 27.0 %all-reduce.2.cloned.1.call-done = bf16[1,32,1024]{2,1,0:T(8,128)(2,1)} async-done(((bf16[1,32,1024]{2,1,0:T(8,128)(2,1)}), bf16[1,32,1024]{2,1,0:T(8,128)(2,1)}) %all-reduce.2.cloned.1.call-update) | async-done | bytes 65552 | tf_op jit(solution)/shard_map/psum | solution.py:110
  92.5 1.1 copy.50
  93.7 0.5 broadcast.215
  94.2 2.3 %reduce.3 = bf16[1024,32]{1,0:T(8,128)(2,1)S(1)} reduce(bf16[1024,1,32]{2,1,0:T(2,128)(2,1)S(1)} %bitcast.149, bf16[]{:T(256)} %broadcast.215), dimensions={1}, to_apply=%bitcast.133.reduce_sub_computation | reduce | bytes 131074
  96.5 0.9 reshape.304
  97.4 5.5 %all-to-all-start.2 = ((bf16[8,2,2048]{2,1,0:T(2,128)(2,1)}), bf16[8,2,2048]{2,1,0:T(2,128)(2,1)S(1)}, u32[]{:S(2)}, u32[]{:S(2)}) async-start(bf16[8,2,2048]{2,1,0:T(2,128)(2,1)} %reshape.304), calls=%async_computation.2 | async-start | bytes 131072 | tf_op jit(solution)/shard_map/all_to_all | solution.py:111
  103.0 6.8 %all-to-all-done.2 = bf16[8,2,2048]{2,1,0:T(2,128)(2,1)S(1)} async-done(((bf16[8,2,2048]{2,1,0:T(2,128)(2,1)}), bf16[8,2,2048]{2,1,0:T(2,128)(2,1)S(1)}, u32[]{:S(2)}, u32[]{:S(2)}) %all-to-all-start.2) | async-done | bytes 65568 | tf_op jit(solution)/shard_map/all_to_all | solution.py:111
  109.8 0.3 reshape.305
  110.1 0.3 copy.51
  110.5 0.7 gather_fusion
  111.2 0.1 fusion.23
  111.3 0.6 add_convert_fusion
  (53 shorter events, 1.3 us)
Async XLA Ops:
  7.2 13.5 %copy-start = (bf16[256,1024]{1,0:T(8,128)(2,1)S(1)}, bf16[256,1024]{1,0:T(8,128)(2,1)}, u32[]{:S(2)}) copy-start(bf16[256,1024]{1,0:T(8,128)(2,1)} %param.30) | copy-start | bytes 1572868
  7.2 2.3 %copy-start.3 = (bf16[8,1024]{1,0:T(8,128)(2,1)S(1)}, bf16[8,1024]{1,0:T(8,128)(2,1)}, u32[]{:S(2)}) copy-start(bf16[8,1024]{1,0:T(8,128)(2,1)} %param.20) | copy-start | bytes 49156
  7.2 6.8 %copy-start.12 = (bf16[1024,128]{1,0:T(8,128)(2,1)S(1)}, bf16[1024,128]{1,0:T(8,128)(2,1)}, u32[]{:S(2)}) copy-start(bf16[1024,128]{1,0:T(8,128)(2,1)} %param.22) | copy-start | bytes 786436
  7.2 8.9 %copy-start.2 = (bf16[1024,256]{1,0:T(8,128)(2,1)S(1)}, bf16[1024,256]{1,0:T(8,128)(2,1)}, u32[]{:S(2)}) copy-start(bf16[1024,256]{1,0:T(8,128)(2,1)} %param.24) | copy-start | bytes 1572868
  7.2 12.6 %copy-start.1 = (f32[8,1,128,256]{3,2,1,0:T(8,128)S(1)}, f32[8,1,128,256]{3,2,1,0:T(8,128)}, u32[]{:S(2)}) copy-start(f32[8,1,128,256]{3,2,1,0:T(8,128)} %param.31) | copy-start | bytes 3145732
  14.0 5.8 %copy-start.11 = (f32[8,1]{0,1:T(1,128)}, f32[8,1]{0,1:T(1,128)S(1)}, u32[]{:S(2)}) copy-start(f32[8,1]{0,1:T(1,128)S(1)} %get-tuple-element.29) | copy-start | bytes 100
  18.3 0.7 copy-start.10
  20.6 0.7 copy-start.13
  38.8 6.0 %copy-start.8 = (s32[64,2]{0,1:T(2,128)S(1)}, s32[64,2]{0,1:T(2,128)}, u32[]{:S(2)}) copy-start(s32[64,2]{0,1:T(2,128)} %param.35) | copy-start | bytes 1540
  38.8 12.5 %all-to-all-start = ((bf16[8,8,128]{2,1,0:T(8,128)(2,1)}), bf16[8,8,128]{2,1,0:T(8,128)(2,1)S(1)}, u32[]{:S(2)}, u32[]{:S(2)}) async-start(bf16[8,8,128]{2,1,0:T(8,128)(2,1)} %constant_dynamic-update-slice_fusion), calls=%async_computation | async-start | bytes 32768 | tf_op jit(solution)/shard_map/all_to_all | solution.py:91
  44.8 47.7 %all-reduce.2.cloned.1.call-start = ((), (), s32[]{:S(2)}) async-start(), calls=%async_computation.3 | async-start | bytes 131072 | tf_op jit(solution)/shard_map/psum | solution.py:110
  51.4 11.0 %copy-start.4 = (bf16[1,1024,128]{2,1,0:T(8,128)(2,1)S(1)}, bf16[1,1024,128]{2,1,0:T(8,128)(2,1)}, u32[]{:S(2)}) copy-start(bf16[1,1024,128]{2,1,0:T(8,128)(2,1)} %param.37) | copy-start | bytes 786436
  61.6 0.7 copy-start.7
  62.3 0.9 copy-start.6
  62.4 1.0 copy-start.5
  64.3 1.2 %copy-start.9 = (f32[64,2]{0,1:T(2,128)S(1)}, f32[64,2]{0,1:T(2,128)}, u32[]{:S(2)}) copy-start(f32[64,2]{0,1:T(2,128)} %param.36) | copy-start | bytes 1540
  97.4 12.4 %all-to-all-start.2 = ((bf16[8,2,2048]{2,1,0:T(2,128)(2,1)}), bf16[8,2,2048]{2,1,0:T(2,128)(2,1)S(1)}, u32[]{:S(2)}, u32[]{:S(2)}) async-start(bf16[8,2,2048]{2,1,0:T(2,128)(2,1)} %reshape.304), calls=%async_computation.2 | async-start | bytes 131072 | tf_op jit(solution)/shard_map/all_to_all | solution.py:111
Sparse Core Ops, SparseCore 0:
  64.4 28.0 all-reduce.1
